TPU v7x, 32 devices: a whole 2x2x4 slice. The times are simulated.
32 devices in a mesh: grp: 2 (over y), kv: 4 (over z), tp: 4 (over x, core).
Axes of the slice: x: 2, y: 2, z: 4, core: 2. Of those that a mesh axis runs over, the one named last changes fastest.
Arguments:
- tokens: bfloat16 [4096, 2048], P(('grp', 'kv'), 'tp'), parts along dimension 0, may hold values from -5400 to 5400, as said below
- gain: bfloat16 [2048], replicated, may hold values from 0.099609375 to 1.8984375
- w_query: bfloat16 [2048, 1024], P(None, 'tp'), may hold values from -1 to 1
- w_key: bfloat16 [2048, 512], P(None, 'tp'), may hold values from -3 to 3
- w_value: bfloat16 [2048, 512], P(None, 'tp'), may hold values from -0.125 to 0.125
- w_out: bfloat16 [1024, 2048], P(None, 'tp'), may hold values from -2 to 2
- select: int32 [32, 32], P(('grp', 'kv')), parts along dimension 0, may hold values from -1 to 63, as said below
Outputs:
- mixed: bfloat16 [4096, 2048], P(('grp', 'kv'), 'tp'), parts along dimension 0
There are 2 independent parts, one for each index of `grp`. A program takes and returns all parts, laid end to end along the dimension named above; an argument that names none is the same for every part. Nothing has to cross between parts.
Inputs may be any that keep to these rules, and one draw needn't show every extreme that they name: Entries of tokens are finite with scales that vary by row and by column. `select`: row b lists distinct key blocks that start no later than query block b ends, or -1 for an empty slot. Every query block lists each key block of its own index of kv up to its own last position. Apart from its own index, the query blocks of one index of kv together list at most 2 distinct key blocks held by any other index; every index but the first lists exactly 2 blocks of the index before it.
All inputs are finite; a program needn't handle non-finite values.
Results may differ from a plain program's by a relative error of at most 0.012.
Values may be sent and summed in bfloat16 or wider, within the bound.
A program may use at most 128 MiB of HBM per device.

v0:
```python
import jax
import jax.numpy as jnp
from jax import lax
from jax.sharding import PartitionSpec as P

HD = 128
QB = 128
KB = 32
CAP = 2


epsilon = 1e-06
theta = 10000.0


def rotary(values, positions):
    head_width = values.shape[-1]
    frequency = theta ** (-jnp.arange(0, head_width, 2, dtype=jnp.float32) / head_width)
    angles = positions.astype(jnp.float32)[:, None] * frequency[None, :]
    cosine = jnp.cos(angles)[:, None, :]
    sine_table = jnp.sin(angles)[:, None, :]
    front_half = values[..., : head_width // 2]
    second = values[..., head_width // 2 :]
    return jnp.concatenate(
        [front_half * cosine - second * sine_table, second * cosine + front_half * sine_table],
        axis=-1,
    )


def per_device(tokens, gain, w_query, w_key, w_value, w_out, select):
    tok_rows = tokens.shape[0]
    model_width = gain.shape[0]
    my_index = lax.axis_index("kv")
    kv_count = lax.axis_size("kv")
    kv_local = w_key.shape[1] // HD
    group_size = w_query.shape[1] // w_key.shape[1]
    gain_f32 = gain.astype(jnp.float32)
    piece_f32 = lax.all_gather(tokens, "tp", axis=1, tiled=True).astype(jnp.float32)
    scaled = (piece_f32 * gain_f32[None, :]).astype(jnp.bfloat16)
    acc_q = jnp.dot(scaled, w_query, preferred_element_type=jnp.float32)
    acc_k = jnp.dot(scaled, w_key, preferred_element_type=jnp.float32)
    acc_v = jnp.dot(scaled, w_value, preferred_element_type=jnp.float32)
    tokens_f32 = tokens.astype(jnp.float32)
    squares = lax.psum(jnp.sum(tokens_f32 * tokens_f32, axis=1), "tp")
    inverse = lax.rsqrt(squares / model_width + epsilon)[:, None]
    positions = my_index * tok_rows + jnp.arange(tok_rows, dtype=jnp.int32)
    queries = rotary((acc_q * inverse).reshape(tok_rows, -1, HD), positions).astype(jnp.bfloat16)
    keys_here = rotary((acc_k * inverse).reshape(tok_rows, kv_local, HD), positions).astype(
        jnp.bfloat16
    )
    values_here = (acc_v * inverse).astype(jnp.bfloat16).reshape(tok_rows, kv_local, HD)
    blocks_dev = tok_rows // KB
    key_blocks = keys_here.reshape(blocks_dev, KB, kv_local, HD)
    value_blocks = values_here.reshape(blocks_dev, KB, kv_local, HD)
    safe_ids = jnp.maximum(select, 0)
    flat_ids = select.reshape(-1)
    owner_of = jnp.where(flat_ids >= 0, flat_ids // blocks_dev, -1)
    peer_ids = jnp.arange(kv_count, dtype=jnp.int32)
    is_match = (owner_of[None, :] == peer_ids[:, None]) & (peer_ids[:, None] != my_index)
    ceiling = jnp.int32(1 << 30)
    lowest = jnp.min(jnp.where(is_match, flat_ids[None, :], ceiling), axis=1)
    highest = jnp.max(jnp.where(is_match, flat_ids[None, :], -1), axis=1)
    wanted = jnp.stack(
        [jnp.where(lowest < ceiling, lowest, -1), jnp.where(highest > lowest, highest, -1)], axis=1
    )
    asked_ids = lax.all_to_all(wanted, "kv", split_axis=0, concat_axis=0, tiled=True)
    local_index = jnp.clip(asked_ids - my_index * blocks_dev, 0, blocks_dev - 1)
    send_k = jnp.take(key_blocks, local_index, axis=0)
    send_v = jnp.take(value_blocks, local_index, axis=0)
    got_k, got_v = (
        lax.all_to_all(send_k, "kv", split_axis=0, concat_axis=0, tiled=True),
        lax.all_to_all(send_v, "kv", split_axis=0, concat_axis=0, tiled=True),
    )
    table_k = jnp.concatenate([key_blocks, got_k.reshape(-1, KB, kv_local, HD)], axis=0)
    table_v = jnp.concatenate([value_blocks, got_v.reshape(-1, KB, kv_local, HD)], axis=0)
    sel_owner = safe_ids // blocks_dev
    pair_ids = jnp.take(wanted, sel_owner, axis=0)
    slot_of = jnp.where(safe_ids == pair_ids[..., 0], 0, 1)
    table_index = jnp.where(
        sel_owner == my_index,
        safe_ids - my_index * blocks_dev,
        blocks_dev + sel_owner * CAP + slot_of,
    )
    query_blocks = select.shape[0]
    chosen_count = select.shape[1]
    keys_sel = jnp.take(table_k, table_index, axis=0).reshape(
        query_blocks, chosen_count * KB, kv_local, HD
    )
    values_sel = jnp.take(table_v, table_index, axis=0).reshape(
        query_blocks, chosen_count * KB, kv_local, HD
    )
    query_rows = queries.reshape(query_blocks, QB, kv_local, group_size, HD)
    scores = jnp.einsum(
        "bqgrd,bkgd->bgrqk", query_rows, keys_sel, preferred_element_type=jnp.float32
    ) * HD ** (-0.5)
    key_pos = (safe_ids[:, :, None] * KB + jnp.arange(KB, dtype=jnp.int32)[None, None, :]).reshape(
        query_blocks, -1
    )
    live_keys = jnp.repeat(select >= 0, KB, axis=1)
    q_pos = positions.reshape(query_blocks, QB)
    allowed = live_keys[:, None, :] & (key_pos[:, None, :] <= q_pos[:, :, None])
    scores = jnp.where(allowed[:, None, None], scores, -jnp.inf)
    row_max = jnp.max(scores, axis=-1, keepdims=True)
    raised = jnp.exp(scores - row_max)
    weights = (raised / jnp.sum(raised, axis=-1, keepdims=True)).astype(jnp.bfloat16)
    attended = jnp.einsum(
        "bgrqk,bkgd->bqgrd", weights, values_sel, preferred_element_type=jnp.float32
    )
    attended = attended.astype(jnp.bfloat16).reshape(tok_rows, -1)
    mixed = jnp.dot(
        lax.all_gather(attended, "tp", axis=1, tiled=True),
        w_out,
        preferred_element_type=jnp.float32,
    )
    return mixed.astype(jnp.bfloat16)


def solution(mesh):
    placed = (
        P(("grp", "kv"), "tp"),
        P(),
        P(None, "tp"),
        P(None, "tp"),
        P(None, "tp"),
        P(None, "tp"),
        P(("grp", "kv"), None),
    )
    return jax.shard_map(
        per_device, mesh=mesh, in_specs=placed, out_specs=P(("grp", "kv"), "tp"), check_vma=False
    )
```

profile of v0, /device:TPU:0, one launch (start us, length us, event | category | flops | bytes accessed | tf_op | source)
XLA Modules:
  0.0 91.5 jit_solution(3641176890367045859)
XLA Ops:
  6.5 0.7 all-gather.3.cloned.1.call-update
  7.3 0.8 reshape.334
  9.1 6.3 %all-to-all-start = ((s32[4,1,2]{2,1,0:T(1,128)}), s32[4,1,2]{2,1,0:T(1,128)S(1)}, u32[]{:S(2)}, u32[]{:S(2)}) async-start(s32[4,1,2]{2,1,0:T(1,128)} %bitcast.31), calls=%async_computation | async-start | bytes 4096 | tf_op jit(solution)/shard_map/all_to_all | solution.py:66
  15.5 0.7 compare_and_fusion.3
  16.2 0.7 convert_element_type.52
  17.0 1.3 %gather_fusion = s32[128,2]{1,0:T(8,128)S(1)} fusion(s32[4,2]{1,0:T(4,128)} %pad_add_fusion, s32[1024]{0:T(1024)S(1)} %pad_clamp_fusion.2), kind=kCustom, calls=%fused_computation.4 | custom fusion | bytes 2560 | tf_op jit(solution)/shard_map/jit(_take)/gather | solution.py:77
  18.4 0.7 compare_and_fusion.1
  19.4 0.7 maximum_multiply_fusion
  20.3 1.2 %multiply_reduce_fusion = f32[512]{0:T(512)S(1)} fusion(bf16[512,512]{1,0:T(8,128)(2,1)} %param.11), kind=kLoop, calls=%fused_computation.26 | loop fusion | flops 785920 | bytes 526336 | tf_op jit(solution)/shard_map/reduce_sum | solution.py:44
  21.5 7.2 %psum.7 = f32[512]{0:T(512)S(1)} all-reduce(f32[512]{0:T(512)S(1)} %multiply_reduce_fusion), channel_id=1, replica_groups=mesh['grp'=2,'kv'=4,'tp'=4] {'tp'}, use_global_device_ids=true, to_apply=%region_1.0 | all-reduce | flops 512 | bytes 4096 | tf_op jit(solution)/shard_map/psum | solution.py:44
  29.3 2.4 %compare_and_fusion = pred[4,128,1024]{1,2,0:T(8,128)(4,1)} fusion(s32[4,128]{1,0:T(4,128)S(1)} %add_add_fusion, s32[4,1024]{1,0:T(4,128)S(1)} %broadcast_add_fusion, pred[4,1024]{1,0:T(4,128)(4,1)S(1)} %and.59), kind=kLoop, calls=%fused_computation.14 | loop fusion | flops 1048576 | bytes 546816 | tf_op jit(solution)/shard_map/and | solution.py:101
  32.1 2.3 %all-gather.3.cloned.1.call-done = bf16[512,2048]{1,0:T(8,128)(2,1)} async-done(((bf16[512,512]{1,0:T(8,128)(2,1)}), bf16[512,2048]{1,0:T(8,128)(2,1)}) %all-gather.3.cloned.1.call-update) | async-done | bytes 2097168 | tf_op jit(solution)/shard_map/all_gather | solution.py:38
  34.3 2.5 %fusion.14 = f32[512,1,128]{2,0,1:T(8,128)S(1)} fusion(bf16[2048,128]{1,0:T(8,128)(2,1)} %param.14, bf16[512,2048]{1,0:T(8,128)(2,1)} %all-gather.3.cloned.1.call-done, f32[2048]{0:T(1024)S(1)} %convert_element_type.52, f32[512]{0:T(512)S(1)} %add_rsqrt_fusion), kind=kOutput, calls=%fused_computation.23 | convolution fusion | flops 271646720 | bytes 2893824 | tf_op jit(solution)/shard_map/dot_general | solution.py:41
  36.9 1.2 %fusion.24 = (bf16[512,1,64]{2,0,1:T(8,128)(2,1)S(1)}, bf16[512,1,64]{2,0,1:T(8,128)(2,1)S(1)}) fusion(f32[512,1,128]{2,0,1:T(8,128)S(1)} %fusion.14, f32[64]{0:T(128)S(1)} %multiply_power_fusion, f32[512]{0:T(512)S(1)} %add_convert_fusion.1), kind=kLoop, calls=%fused_computation.36 | loop fusion | flops 294912 | bytes 395520 | tf_op jit(solution)/shard_map/convert.7
  38.1 0.7 fusion.18
  40.1 0.7 broadcast_select_fusion.2
  40.8 4.6 %all-to-all-start.2 = ((bf16[4,2,32,1,128]{4,2,1,3,0:T(8,128)(2,1)}), bf16[4,2,32,1,128]{4,2,1,3,0:T(8,128)(2,1)S(1)}, u32[]{:S(2)}, u32[]{:S(2)}) async-start(bf16[4,2,32,1,128]{4,2,1,3,0:T(8,128)(2,1)} %get-tuple-element.26), calls=%async_computation.2 | async-start | bytes 131072 | tf_op jit(solution)/shard_map/all_to_all | solution.py:71
  45.5 2.4 %fusion.8 = f32[512,256]{0,1:T(8,128)S(1)} fusion(bf16[2048,256]{1,0:T(8,128)(2,1)S(1)} %copy-done.5, bf16[512,2048]{1,0:T(8,128)(2,1)} %all-gather.3.cloned.1.call-done, f32[2048]{0:T(1024)S(1)} %convert_element_type.52, f32[512]{0:T(512)S(1)} %add_rsqrt_fusion), kind=kOutput, calls=%fused_computation.19 | convolution fusion | flops 540147712 | bytes 3680256 | tf_op jit(solution)/shard_map/dot_general | solution.py:40
  48.0 0.9 copy.91
  48.9 0.9 copy.92
  49.8 1.5 %all-to-all-done.2 = bf16[4,2,32,1,128]{4,2,1,3,0:T(8,128)(2,1)S(1)} async-done(((bf16[4,2,32,1,128]{4,2,1,3,0:T(8,128)(2,1)}), bf16[4,2,32,1,128]{4,2,1,3,0:T(8,128)(2,1)S(1)}, u32[]{:S(2)}, u32[]{:S(2)}) %all-to-all-start.2) | async-done | bytes 65568 | tf_op jit(solution)/shard_map/all_to_all | solution.py:71
  51.2 3.6 %all-to-all-start.1 = ((bf16[4,2,32,1,128]{4,2,1,3,0:T(8,128)(2,1)}), bf16[4,2,32,1,128]{4,2,1,3,0:T(8,128)(2,1)S(1)}, u32[]{:S(2)}, u32[]{:S(2)}) async-start(bf16[4,2,32,1,128]{4,2,1,3,0:T(8,128)(2,1)} %get-tuple-element.27), calls=%async_computation.1 | async-start | bytes 131072 | tf_op jit(solution)/shard_map/all_to_all | solution.py:72
  55.0 5.6 %all-to-all-done.1 = bf16[4,2,32,1,128]{4,2,1,3,0:T(8,128)(2,1)S(1)} async-done(((bf16[4,2,32,1,128]{4,2,1,3,0:T(8,128)(2,1)}), bf16[4,2,32,1,128]{4,2,1,3,0:T(8,128)(2,1)S(1)}, u32[]{:S(2)}, u32[]{:S(2)}) %all-to-all-start.1) | async-done | bytes 65568 | tf_op jit(solution)/shard_map/all_to_all | solution.py:72
  60.6 0.8 gather_fusion.2
  61.4 0.8 gather_fusion.4
  62.5 0.7 copy-done.1
  63.3 0.8 fusion.1
  64.2 1.0 %fusion = f32[4,2,128]{2,1,0:T(2,128)S(1)} fusion(f32[4,1024,128,2]{2,1,3,0:T(8,128)S(1)} %get-tuple-element.29, f32[4,2,128]{2,1,0:T(2,128)S(1)} %get-tuple-element.28, pred[4,128,1024]{1,2,0:T(8,128)(4,1)S(1)} %copy-done.1), kind=kLoop, calls=%fused_computation.9 | loop fusion | flops 4193280 | bytes 4726784 | tf_op jit(solution)/shard_map/reduce_sum | solution.py:105
  65.1 1.4 %fusion.15 = bf16[4,128,1,2,128]{1,4,3,0,2:T(8,128)(2,1)S(1)} fusion(bf16[4,1024,128,1]{2,1,3,0:T(8,128)(2,1)S(1)} %bitcast.96, f32[4,2,128]{2,1,0:T(2,128)S(1)} %fusion, f32[4,2,128]{2,1,0:T(2,128)S(1)} %get-tuple-element.28, f32[4,1024,128,2]{2,1,3,0:T(8,128)S(1)} %get-tuple-element.29, pred[4,128,1024]{1,2,0:T(8,128)(4,1)S(1)} %copy-done.1), kind=kOutput, calls=%fused_computation.24 | convolution fusion | flops 273809408 | bytes 6037504 | tf_op jit(solution)/shard_map/bgrqk,bkgd->bqgrd/dot_general | solution.py:106
  66.7 0.7 copy.107
  67.4 14.5 %all-gather.5.cloned.1.call-done = bf16[512,1024]{1,0:T(8,128)(2,1)} async-done(((bf16[512,256]{1,0:T(8,128)(2,1)}), bf16[512,1024]{1,0:T(8,128)(2,1)}) %all-gather.5.cloned.1.call-update) | async-done | bytes 1048592 | tf_op jit(solution)/shard_map/all_gather | solution.py:111
  82.0 2.7 %convolution_convert_fusion = bf16[512,512]{1,0:T(8,128)(2,1)} fusion(bf16[512,1024]{1,0:T(8,128)(2,1)} %all-gather.5.cloned.1.call-done, bf16[1024,512]{1,0:T(8,128)(2,1)S(1)} %copy-done), kind=kOutput, calls=%fused_computation.18 | convolution fusion | flops 537133056 | bytes 2621440 | tf_op jit(solution)/shard_map/dot_general | solution.py:110
  (57 shorter events, 4.9 us)
Async XLA Ops:
  6.5 75.4 %copy-start = (bf16[1024,512]{1,0:T(8,128)(2,1)S(1)}, bf16[1024,512]{1,0:T(8,128)(2,1)}, u32[]{:S(2)}) copy-start(bf16[1024,512]{1,0:T(8,128)(2,1)} %param.16) | copy-start | bytes 3145732
  6.5 27.8 %all-gather.3.cloned.1.call-start = ((), (), s32[]{:S(2)}) async-start(), calls=%async_computation.3 | async-start | bytes 2621440 | tf_op jit(solution)/shard_map/all_gather | solution.py:38
  9.1 22.6 %all-to-all-start = ((s32[4,1,2]{2,1,0:T(1,128)}), s32[4,1,2]{2,1,0:T(1,128)S(1)}, u32[]{:S(2)}, u32[]{:S(2)}) async-start(s32[4,1,2]{2,1,0:T(1,128)} %bitcast.31), calls=%async_computation | async-start | bytes 4096 | tf_op jit(solution)/shard_map/all_to_all | solution.py:66
  32.1 13.4 %copy-start.5 = (bf16[2048,256]{1,0:T(8,128)(2,1)S(1)}, bf16[2048,256]{1,0:T(8,128)(2,1)}, u32[]{:S(2)}) copy-start(bf16[2048,256]{1,0:T(8,128)(2,1)} %param.13) | copy-start | bytes 3145732
  34.3 3.8 %copy-start.4 = (bf16[512,2048]{1,0:T(8,128)(2,1)S(1)}, bf16[512,2048]{1,0:T(8,128)(2,1)}, u32[]{:S(2)}) copy-start(bf16[512,2048]{1,0:T(8,128)(2,1)} %all-gather.3.cloned.1.call-done) | copy-start | bytes 6291460
  34.3 3.8 %copy-start.6 = (bf16[2048,128]{1,0:T(8,128)(2,1)S(1)}, bf16[2048,128]{1,0:T(8,128)(2,1)}, u32[]{:S(2)}) copy-start(bf16[2048,128]{1,0:T(8,128)(2,1)} %param.15) | copy-start | bytes 1572868
  40.8 10.4 %all-to-all-start.2 = ((bf16[4,2,32,1,128]{4,2,1,3,0:T(8,128)(2,1)}), bf16[4,2,32,1,128]{4,2,1,3,0:T(8,128)(2,1)S(1)}, u32[]{:S(2)}, u32[]{:S(2)}) async-start(bf16[4,2,32,1,128]{4,2,1,3,0:T(8,128)(2,1)} %get-tuple-element.26), calls=%async_computation.2 | async-start | bytes 131072 | tf_op jit(solution)/shard_map/all_to_all | solution.py:71
  51.2 9.4 %all-to-all-start.1 = ((bf16[4,2,32,1,128]{4,2,1,3,0:T(8,128)(2,1)}), bf16[4,2,32,1,128]{4,2,1,3,0:T(8,128)(2,1)S(1)}, u32[]{:S(2)}, u32[]{:S(2)}) async-start(bf16[4,2,32,1,128]{4,2,1,3,0:T(8,128)(2,1)} %get-tuple-element.27), calls=%async_computation.1 | async-start | bytes 131072 | tf_op jit(solution)/shard_map/all_to_all | solution.py:72
  54.9 27.1 %all-gather.5.cloned.1.call-start = ((), (), s32[]{:S(2)}) async-start(), calls=%async_computation.4 | async-start | bytes 1310720 | tf_op jit(solution)/shard_map/all_gather | solution.py:111
  62.2 1.0 %copy-start.1 = (pred[4,128,1024]{1,2,0:T(8,128)(4,1)S(1)}, pred[4,128,1024]{1,2,0:T(8,128)(4,1)}, u32[]{:S(2)}) copy-start(pred[4,128,1024]{1,2,0:T(8,128)(4,1)} %compare_and_fusion) | copy-start | bytes 1572868
  62.2 1.1 %copy-start.2 = (bf16[4,128,2,64]{3,1,2,0:T(8,128)(2,1)S(1)}, bf16[4,128,2,64]{3,1,2,0:T(8,128)(2,1)}, u32[]{:S(2)}) copy-start(bf16[4,128,2,64]{3,1,2,0:T(8,128)(2,1)} %copy.91) | copy-start | bytes 393220
  62.2 1.2 %copy-start.3 = (bf16[4,128,2,64]{3,1,2,0:T(8,128)(2,1)S(1)}, bf16[4,128,2,64]{3,1,2,0:T(8,128)(2,1)}, u32[]{:S(2)}) copy-start(bf16[4,128,2,64]{3,1,2,0:T(8,128)(2,1)} %copy.92) | copy-start | bytes 393220
Sparse Core Ops, SparseCore 0:
  8.9 25.4 all-gather.2
  67.6 14.3 all-gather.4
where the time goes:
time: 92.2 us; the launch traced here: 91.5 us
  waiting for transfers between devices  24.6 us (27%)
  starting transfers between devices  14.6 us (16%)
  between operations  13.6 us (15%)
  other arithmetic  11.4 us (12%)
  matrix products  10.5 us (11%)
  local copies, waits for them, and re-layouts  9.64 us (10%)
  blocking collectives  7.17 us (8%)
    all_gather x1, waiting for transfers between devices, per_device(): lax.all_gather(attended, 'tp', axis=1, tiled=True)  14.5 us
    psum x1, blocking collectives, per_device(): squares = lax.psum(jnp.sum(tokens_f32 * tokens_f32, axis=1), 'tp')  7.17 us
    all_to_all x1, starting transfers between devices, per_device(): lax.all_to_all(wanted, 'kv', split_axis=0, concat_axis=0, tiled=True)  6.35 us
    all_to_all x1, waiting for transfers between devices, per_device(): lax.all_to_all(send_v, 'kv', split_axis=0, concat_axis=0, tiled=True)  5.63 us
    all_to_all x1, starting transfers between devices, per_device(): lax.all_to_all(send_k, 'kv', split_axis=0, concat_axis=0, tiled=True)  4.65 us
    all_to_all x1, starting transfers between devices, per_device(): lax.all_to_all(send_v, 'kv', split_axis=0, concat_axis=0, tiled=True)  3.63 us
    dot_general x1, matrix products, per_device(): jnp.dot(lax.all_gather(attended, 'tp', axis=1, tiled=True), w_out, prefer...  2.73 us
    dot_general x1, matrix products, per_device(): acc_k = jnp.dot(scaled, w_key, preferred_element_type=jnp.float32)  2.54 us
  transfers between devices with their start and end apart: 5, of which 4 were waited for; matrix products, arithmetic and copies ran while one was open for 17% of the time, Pallas kernels for 0%

commit v1 on v0

v1 whole, which is shorter than its diff:
```python
import functools

import jax
import jax.numpy as jnp
from jax import lax
from jax.experimental import pallas as pl
from jax.experimental.pallas import tpu as pltpu
from jax.sharding import PartitionSpec as P

HD = 128
QB = 128
KB = 32
CAP = 2

epsilon = 1e-06
theta = 10000.0
MESH = pl.DeviceIdType.MESH
F32 = jnp.float32
BF16 = jnp.bfloat16
LOW = -1e30


def loop(count, body):
    if count <= 4:
        for i in range(count):
            body(i)
    else:
        lax.fori_loop(0, count, lambda i, c: (body(i), c)[1], 0)


def kernel(
    tp, n_kv,
    tokens, gain, w_query, w_key, w_value, w_out, select,
    out,
    tok, att, w_in, w_o, q_s, kv_s, hot_s, cos_s, sin_s, o_s, m_s, l_s,
    sel_all, send_kv, recv_kv, bias_s,
    local_sem, tok_send, tok_recv, fwd_send, fwd_recv, mate_send, mate_recv,
    sel_send, sel_recv, kv_send, kv_recv,
    att_send, att_recv, afwd_send, afwd_recv, amate_send, amate_recv,
):
    rows, cols = tokens.shape
    width = tp * cols
    blocks = rows // QB
    groups = tp // 2
    me_tp = lax.axis_index("tp")
    me_kv = lax.axis_index("kv")
    side = lax.rem(me_tp, 2)
    group = lax.div(me_tp, 2)
    mate = group * 2 + 1 - side
    nq, nk = w_query.shape[1], w_key.shape[1]
    heads, kv_heads = nq // HD, nk // HD
    per = heads // kv_heads
    dev_blocks = rows // KB
    spec_rows = CAP * KB

    def other(i):
        return lax.rem(group + 1 + i, groups) * 2 + side

    copies = [
        pltpu.make_async_copy(tokens, tok.at[me_tp], local_sem.at[0]),
        pltpu.make_async_copy(w_query, w_in.at[:, pl.ds(0, nq)], local_sem.at[1]),
        pltpu.make_async_copy(w_key, w_in.at[:, pl.ds(nq, nk)], local_sem.at[2]),
        pltpu.make_async_copy(w_value, w_in.at[:, pl.ds(nq + nk, nk)], local_sem.at[3]),
        pltpu.make_async_copy(w_out, w_o, local_sem.at[4]),
    ]
    for copy in copies:
        copy.start()

    barrier = pltpu.get_barrier_semaphore()
    pl.semaphore_signal(barrier, inc=1, device_id={"tp": mate}, device_id_type=MESH)
    for i in range(groups - 1):
        pl.semaphore_signal(barrier, inc=1, device_id={"tp": other(i)}, device_id_type=MESH)

    def greet(i):
        peer = lax.rem(me_kv + 1 + i, n_kv)
        pl.semaphore_signal(barrier, inc=1, device_id={"kv": peer}, device_id_type=MESH)

    loop(n_kv - 1, greet)
    pl.semaphore_wait(barrier, groups + n_kv - 1)

    def piece(ref, slot, b):
        return ref.at[slot, pl.ds(b * QB, QB), :]

    def tok_copy(i, b):
        return pltpu.make_async_remote_copy(
            src_ref=tokens.at[pl.ds(b * QB, QB), :], dst_ref=piece(tok, me_tp, b),
            send_sem=tok_send.at[i, b], recv_sem=tok_recv.at[groups - 2 - i, b],
            device_id={"tp": other(i)}, device_id_type=MESH)

    def tok_wait(i, b):
        return pltpu.make_async_remote_copy(
            src_ref=tokens.at[pl.ds(b * QB, QB), :], dst_ref=piece(tok, other(i), b),
            send_sem=tok_send.at[i, b], recv_sem=tok_recv.at[i, b],
            device_id={"tp": other(i)}, device_id_type=MESH)

    def mate_copy(b):
        return pltpu.make_async_remote_copy(
            src_ref=tokens.at[pl.ds(b * QB, QB), :], dst_ref=piece(tok, me_tp, b),
            send_sem=mate_send.at[b], recv_sem=mate_recv.at[b],
            device_id={"tp": mate}, device_id_type=MESH)

    def fwd_copy(i, b):
        return pltpu.make_async_remote_copy(
            src_ref=piece(tok, other(i), b), dst_ref=piece(tok, other(i), b),
            send_sem=fwd_send.at[i, b], recv_sem=fwd_recv.at[i, b],
            device_id={"tp": mate}, device_id_type=MESH)

    for b in range(blocks):
        for i in range(groups - 1):
            tok_copy(i, b).start()
        mate_copy(b).start()

    def sel_copy(peer):
        return pltpu.make_async_remote_copy(
            src_ref=select, dst_ref=sel_all.at[me_kv],
            send_sem=sel_send.at[peer], recv_sem=sel_recv.at[me_kv],
            device_id={"kv": peer}, device_id_type=MESH)

    def sel_wait(peer):
        return pltpu.make_async_remote_copy(
            src_ref=select, dst_ref=sel_all.at[peer],
            send_sem=sel_send.at[peer], recv_sem=sel_recv.at[peer],
            device_id={"kv": peer}, device_id_type=MESH)

    def send_select(peer):
        @pl.when(peer < me_kv)
        def _():
            sel_copy(peer).start()

    loop(n_kv - 1, send_select)

    lane = lax.broadcasted_iota(jnp.int32, (1, HD), 1)
    half = HD // 2
    frequency = jnp.exp(
        lax.rem(lane, half).astype(F32) * (-2.0 / HD) * jnp.log(F32(theta)))
    for b in range(blocks):
        place = me_kv * rows + b * QB + lax.broadcasted_iota(jnp.int32, (QB, HD), 0)
        angle = place.astype(F32) * frequency
        cos_s[b * QB:(b + 1) * QB, :] = jnp.cos(angle)
        sine = jnp.sin(angle)
        sin_s[b * QB:(b + 1) * QB, :] = jnp.where(lane < half, -sine, sine)

    chunks, chunk_owners, chunk_keys = bias_s.shape[0], recv_kv.shape[1], bias_s.shape[2]
    listed = select[...]

    def bounds(ids, owner):
        first = owner * dev_blocks
        inside = (ids >= first) & (ids < first + dev_blocks)
        low = jnp.min(jnp.where(inside, ids, 1 << 20), axis=(0, 1), keepdims=True)
        high = jnp.max(jnp.where(inside, ids, -1), axis=(0, 1), keepdims=True)
        return low, high

    key_lane = lax.broadcasted_iota(jnp.int32, (1, chunk_keys), 1)

    def make_bias(c):
        bias = jnp.full((blocks, chunk_keys), LOW, F32)
        for w in range(chunk_owners):
            owner = c * chunk_owners + w
            low, high = bounds(listed, owner)
            has_low = jnp.max(jnp.where(listed == low, 1, 0), axis=1, keepdims=True)
            has_high = jnp.max(
                jnp.where((listed == high) & (high > low), 1, 0), axis=1, keepdims=True)
            start = w * spec_rows
            in_low = (key_lane >= start) & (key_lane < start + KB)
            in_high = (key_lane >= start + KB) & (key_lane < start + spec_rows)
            hit = jnp.where(in_low, has_low, 0) + jnp.where(in_high, has_high, 0)
            hit = jnp.where(owner < me_kv, hit, 0)
            bias = jnp.where(hit > 0, 0.0, bias)

            @pl.when(owner >= me_kv)
            def _():
                recv_kv[c, w] = jnp.zeros(recv_kv.shape[2:], recv_kv.dtype)

        bias_s[c] = bias

    loop(chunks, make_bias)

    def make_hot(p):
        peer = p + 1

        @pl.when(peer > me_kv)
        def _():
            sel_wait(peer).wait_recv()
            low, high = bounds(sel_all[peer], me_kv)
            row = lax.broadcasted_iota(jnp.int32, (spec_rows, 1), 0)
            want = jnp.where(row < KB, low, high) * KB + lax.rem(row, KB) - me_kv * rows
            col = lax.broadcasted_iota(jnp.int32, (spec_rows, rows), 1)
            hot_s[peer] = jnp.where(col == want, 1.0, 0.0).astype(BF16)

    loop(n_kv - 1, make_hot)

    for copy in copies[:4]:
        copy.wait()

    def add_part(slot, b, acc, squares):
        part = tok[slot, pl.ds(b * QB, QB), :].astype(F32)
        factor = gain[:, pl.ds(pl.multiple_of(slot * cols, cols), cols)].astype(F32)
        scaled = (part * factor).astype(BF16)
        weight = w_in[pl.ds(pl.multiple_of(slot * cols, cols), cols), :]
        acc = acc + jnp.dot(scaled, weight, preferred_element_type=F32)
        squares = squares + jnp.sum(part * part, axis=1, keepdims=True)
        return acc, squares

    def rotate(x, b):
        cosine = cos_s[b * QB:(b + 1) * QB, :]
        sine = sin_s[b * QB:(b + 1) * QB, :]
        return x * cosine + pltpu.roll(x, half, 1) * sine

    factor2 = HD ** (-0.5) * 1.4426950408889634

    def project(b):
        acc = jnp.zeros((QB, nq + 2 * nk), F32)
        squares = jnp.zeros((QB, 1), F32)
        acc, squares = add_part(me_tp, b, acc, squares)
        mate_copy(b).wait_recv()
        acc, squares = add_part(mate, b, acc, squares)
        for i in range(groups - 1):
            tok_wait(i, b).wait_recv()
            fwd_copy(i, b).start()
            acc, squares = add_part(other(i), b, acc, squares)
        for i in range(groups - 1):
            fwd_copy(i, b).wait_recv()
            far = lax.rem(group + 1 + i, groups) * 2 + 1 - side
            acc, squares = add_part(far, b, acc, squares)
        inverse = lax.rsqrt(squares / width + epsilon)
        acc = acc * inverse
        here = slice(b * QB, (b + 1) * QB)
        for h in range(heads):
            q_s[h, here, :] = rotate(acc[:, h * HD:(h + 1) * HD], b).astype(BF16)
        for g in range(kv_heads):
            at = nq + g * HD
            kv_s[here, g * HD:(g + 1) * HD] = rotate(acc[:, at:at + HD], b).astype(BF16)
        kv_s[here, nk:] = acc[:, nq + nk:].astype(BF16)

    def head_rows(b, g):
        parts = [q_s[g * per + r, b * QB:(b + 1) * QB, :] for r in range(per)]
        return jnp.concatenate(parts, axis=0)

    def near(b):
        count = (b + 1) * QB
        for g in range(kv_heads):
            here = slice(g * HD, (g + 1) * HD)
            there = slice(nk + g * HD, nk + (g + 1) * HD)
            scores = lax.dot_general(
                head_rows(b, g), kv_s[0:count, here], (((1,), (1,)), ((), ())),
                preferred_element_type=F32) * factor2
            row = lax.rem(lax.broadcasted_iota(jnp.int32, scores.shape, 0), QB) + b * QB
            col = lax.broadcasted_iota(jnp.int32, scores.shape, 1)
            scores = jnp.where(col <= row, scores, LOW)
            top = jnp.max(scores, axis=1, keepdims=True)
            raised = jnp.exp2(scores - top)
            m_s[b, g] = jnp.broadcast_to(top, m_s.shape[2:])
            l_s[b, g] = jnp.broadcast_to(jnp.sum(raised, axis=1, keepdims=True), l_s.shape[2:])
            o_s[b, g] = jnp.dot(
                raised.astype(BF16), kv_s[0:count, there], preferred_element_type=F32)

    def add_far(c, b):
        for g in range(kv_heads):
            here = slice(g * HD, (g + 1) * HD)
            there = slice(nk + g * HD, nk + (g + 1) * HD)
            far_k = jnp.concatenate(
                [recv_kv[c, w, :, here] for w in range(chunk_owners)], axis=0)
            far_v = jnp.concatenate(
                [recv_kv[c, w, :, there] for w in range(chunk_owners)], axis=0)
            scores = lax.dot_general(
                head_rows(b, g), far_k, (((1,), (1,)), ((), ())),
                preferred_element_type=F32) * factor2
            hit = bias_s[c, b:b + 1, :] == 0.0
            scores = jnp.where(hit, scores, LOW)
            before = m_s[b, g]
            top = jnp.maximum(before, jnp.max(scores, axis=1, keepdims=True))
            keep = jnp.exp2(before - top)
            raised = jnp.exp2(scores - top[:, 0:1])
            m_s[b, g] = top
            l_s[b, g] = l_s[b, g] * keep + jnp.sum(raised, axis=1, keepdims=True)
            o_s[b, g] = o_s[b, g] * keep + jnp.dot(
                raised.astype(BF16), far_v, preferred_element_type=F32)

    def kv_copy(peer):
        return pltpu.make_async_remote_copy(
            src_ref=send_kv.at[peer],
            dst_ref=recv_kv.at[lax.div(me_kv, chunk_owners), lax.rem(me_kv, chunk_owners)],
            send_sem=kv_send.at[peer], recv_sem=kv_recv.at[me_kv],
            device_id={"kv": peer}, device_id_type=MESH)

    def kv_wait(peer):
        return pltpu.make_async_remote_copy(
            src_ref=send_kv.at[peer],
            dst_ref=recv_kv.at[lax.div(peer, chunk_owners), lax.rem(peer, chunk_owners)],
            send_sem=kv_send.at[peer], recv_sem=kv_recv.at[peer],
            device_id={"kv": peer}, device_id_type=MESH)

    def send_blocks(p):
        peer = p + 1

        @pl.when(peer > me_kv)
        def _():
            send_kv[peer] = jnp.dot(
                hot_s[peer], kv_s[...], preferred_element_type=F32).astype(BF16)
            kv_copy(peer).start()

    for b in range(blocks):
        project(b)
        if b == blocks - 1:
            loop(n_kv - 1, send_blocks)
        near(b)

    def take_blocks(peer):
        @pl.when(peer < me_kv)
        def _():
            kv_wait(peer).wait_recv()

    loop(n_kv - 1, take_blocks)
    copies[4].wait()

    def att_copy(i, b):
        return pltpu.make_async_remote_copy(
            src_ref=piece(att, me_tp, b), dst_ref=piece(att, me_tp, b),
            send_sem=att_send.at[i, b], recv_sem=att_recv.at[groups - 2 - i, b],
            device_id={"tp": other(i)}, device_id_type=MESH)

    def att_wait(i, b):
        return pltpu.make_async_remote_copy(
            src_ref=piece(att, me_tp, b), dst_ref=piece(att, other(i), b),
            send_sem=att_send.at[i, b], recv_sem=att_recv.at[i, b],
            device_id={"tp": other(i)}, device_id_type=MESH)

    def amate_copy(b):
        return pltpu.make_async_remote_copy(
            src_ref=piece(att, me_tp, b), dst_ref=piece(att, me_tp, b),
            send_sem=amate_send.at[b], recv_sem=amate_recv.at[b],
            device_id={"tp": mate}, device_id_type=MESH)

    def amate_wait(b):
        return pltpu.make_async_remote_copy(
            src_ref=piece(att, me_tp, b), dst_ref=piece(att, mate, b),
            send_sem=amate_send.at[b], recv_sem=amate_recv.at[b],
            device_id={"tp": mate}, device_id_type=MESH)

    def afwd_copy(i, b):
        return pltpu.make_async_remote_copy(
            src_ref=piece(att, other(i), b), dst_ref=piece(att, other(i), b),
            send_sem=afwd_send.at[i, b], recv_sem=afwd_recv.at[i, b],
            device_id={"tp": mate}, device_id_type=MESH)

    for b in range(blocks):
        loop(chunks, functools.partial(add_far, b=b))
        for g in range(kv_heads):
            done = (o_s[b, g] / l_s[b, g]).astype(BF16)
            for r in range(per):
                h = g * per + r
                att[me_tp, pl.ds(b * QB, QB), h * HD:(h + 1) * HD] = (
                    done[r * QB:(r + 1) * QB])
        for i in range(groups - 1):
            att_copy(i, b).start()
        amate_copy(b).start()

    def mix(slot, b):
        weight = w_o[pl.ds(pl.multiple_of(slot * nq, nq), nq), :]
        return jnp.dot(att[slot, pl.ds(b * QB, QB), :], weight, preferred_element_type=F32)

    def relay(b):
        for i in range(groups - 1):
            att_wait(i, b).wait_recv()
            afwd_copy(i, b).start()

    relay(0)
    for b in range(blocks):
        amate_wait(b).wait_recv()
        total = mix(me_tp, b) + mix(mate, b)
        for i in range(groups - 1):
            total = total + mix(other(i), b)
        if b + 1 < blocks:
            relay(b + 1)
        for i in range(groups - 1):
            afwd_copy(i, b).wait_recv()
            far = lax.rem(group + 1 + i, groups) * 2 + 1 - side
            total = total + mix(far, b)
        out[b * QB:(b + 1) * QB, :] = total.astype(out.dtype)

    for b in range(blocks):
        mate_copy(b).wait_send()
        amate_copy(b).wait_send()
        for i in range(groups - 1):
            tok_copy(i, b).wait_send()
            fwd_copy(i, b).wait_send()
            att_copy(i, b).wait_send()
            afwd_copy(i, b).wait_send()

    def finish(p):
        @pl.when(p < me_kv)
        def _():
            sel_copy(p).wait_send()

        @pl.when(p + 1 > me_kv)
        def _():
            kv_copy(p + 1).wait_send()

    loop(n_kv - 1, finish)


def per_device(tp, n_kv, tokens, gain, w_query, w_key, w_value, w_out, select):
    rows, cols = tokens.shape
    depth, nq = w_query.shape
    nk = w_key.shape[1]
    heads, kv_heads = nq // HD, nk // HD
    per = heads // kv_heads
    blocks = rows // QB
    groups = tp // 2
    owners = n_kv - 1
    chunk_owners = max(c for c in (1, 2, 3, 4) if owners % c == 0)
    chunks = owners // chunk_owners
    spec_rows = CAP * KB
    dma = pltpu.SemaphoreType.DMA
    anywhere = pl.BlockSpec(memory_space=pl.ANY)
    fast = pl.BlockSpec(memory_space=pltpu.VMEM)
    return pl.pallas_call(
        functools.partial(kernel, tp, n_kv),
        out_shape=jax.ShapeDtypeStruct((rows, w_out.shape[1]), jnp.bfloat16),
        in_specs=[anywhere, fast, anywhere, anywhere, anywhere, anywhere, fast],
        out_specs=fast,
        scratch_shapes=[
            pltpu.VMEM((tp, rows, cols), BF16),
            pltpu.VMEM((tp, rows, nq), BF16),
            pltpu.VMEM((depth, nq + 2 * nk), BF16),
            pltpu.VMEM(w_out.shape, BF16),
            pltpu.VMEM((heads, rows, HD), BF16),
            pltpu.VMEM((rows, 2 * nk), BF16),
            pltpu.VMEM((n_kv, spec_rows, rows), BF16),
            pltpu.VMEM((rows, HD), F32),
            pltpu.VMEM((rows, HD), F32),
            pltpu.VMEM((blocks, kv_heads, per * QB, HD), F32),
            pltpu.VMEM((blocks, kv_heads, per * QB, HD), F32),
            pltpu.VMEM((blocks, kv_heads, per * QB, HD), F32),
            pltpu.VMEM((n_kv,) + select.shape, jnp.int32),
            pltpu.VMEM((n_kv, spec_rows, 2 * nk), BF16),
            pltpu.VMEM((chunks, chunk_owners, spec_rows, 2 * nk), BF16),
            pltpu.VMEM((chunks, blocks, chunk_owners * spec_rows), F32),
            dma((5,)),
            dma((groups - 1, blocks)),
            dma((groups - 1, blocks)),
            dma((groups - 1, blocks)),
            dma((groups - 1, blocks)),
            dma((blocks,)),
            dma((blocks,)),
            dma((n_kv,)),
            dma((n_kv,)),
            dma((n_kv,)),
            dma((n_kv,)),
            dma((groups - 1, blocks)),
            dma((groups - 1, blocks)),
            dma((groups - 1, blocks)),
            dma((groups - 1, blocks)),
            dma((blocks,)),
            dma((blocks,)),
        ],
        compiler_params=pltpu.CompilerParams(
            collective_id=0, has_side_effects=True, vmem_limit_bytes=60 * 1024 * 1024),
    )(tokens, gain.reshape(1, -1), w_query, w_key, w_value, w_out, select)


def solution(mesh):
    placed = (
        P(("grp", "kv"), "tp"),
        P(),
        P(None, "tp"),
        P(None, "tp"),
        P(None, "tp"),
        P(None, "tp"),
        P(("grp", "kv"), None),
    )
    return jax.shard_map(
        functools.partial(per_device, mesh.shape["tp"], mesh.shape["kv"]),
        mesh=mesh, in_specs=placed, out_specs=P(("grp", "kv"), "tp"), check_vma=False
    )
```

time: 92.2 us -> 35.7 us (0.39)
  the two profiles are of different devices: /device:TPU:0 before, /device:TPU:27 now
where the time goes in v1:
time: 35.7 us; the launch traced here: 35.4 us
  Pallas kernels  32.3 us (90%)
  local copies, waits for them, and re-layouts  3.16 us (9%)
    pallas_call x1, Pallas kernels, per_device(): pl.pallas_call(functools.partial(kernel, tp, n_kv), out_shape=jax.ShapeDt...  32.3 us
    unnamed x1, local copies, waits for them, and re-layouts  1.87 us
    reshape x1, local copies, waits for them, and re-layouts, per_device(): gain.reshape(1, -1)  1.29 us

profile of v1, /device:TPU:27, one launch (start us, length us, event | category | flops | bytes accessed | tf_op | source)
XLA Modules:
  0.0 35.4 jit_solution(5752112501628076408)
XLA Ops:
  0.0 1.3 %reshape.3.gain = bf16[1,2048]{1,0:T(2,128)(2,1)} reshape(bf16[2048]{0:T(1024)(128)(2,1)} %param.8) | data formatting | bytes 8192 | tf_op jit(solution)/shard_map/reshape | solution.py:459
  1.3 32.3 %shard_map.73 = bf16[512,512]{1,0:T(8,128)(2,1)} custom-call(bf16[512,512]{1,0:T(8,128)(2,1)} %tokens.1, bf16[1,2048]{1,0:T(2,128)(2,1)} %reshape.3.gain, bf16[2048,256]{1,0:T(8,128)(2,1)} %w_query.1, bf16[2048,128]{1,0:T(8,128)(2,1)} %w_key.1, bf16[2048,128]{1,0:T(8,128)(2,1)} %w_value.1, bf16[1024,512]{1,0:T(8,128)(2,1)} %w_out.1, s32[4,32]{1,0:T(4,128)} %select.1), custom_call_target="tpu_custom_call" | custom-call | tf_op jit(solution)/shard_map/pallas_call | solution.py:417
  33.6 1.9 %copy.9 = bf16[512,512]{1,0:T(8,128)(2,1)} copy(bf16[512,512]{1,0:T(8,128)(2,1)} %shard_map.73) | data formatting | bytes 1048576

commit v2 on v1

--- a/solution.py
+++ b/solution.py
@@ -30,12 +30,12 @@
 
 def kernel(
     tp, n_kv,
-    tokens, gain, w_query, w_key, w_value, w_out, select,
+    tokens, gain_in, w_query, w_key, w_value, w_out, select_in,
     out,
-    tok, att, w_in, w_o, q_s, kv_s, hot_s, cos_s, sin_s, o_s, m_s, l_s,
+    gain, select,    tok, att, w_in, w_o, q_s, kv_s, hot_s, cos_s, sin_s, o_s, m_s, l_s,
     sel_all, send_kv, recv_kv, bias_s,
     local_sem, tok_send, tok_recv, fwd_send, fwd_recv, mate_send, mate_recv,
-    sel_send, sel_recv, kv_send, kv_recv,
+    sel_send, sel_recv, chain_sem, kv_send, kv_recv,
     att_send, att_recv, afwd_send, afwd_recv, amate_send, amate_recv,
 ):
     rows, cols = tokens.shape
@@ -62,6 +62,8 @@
         pltpu.make_async_copy(w_key, w_in.at[:, pl.ds(nq, nk)], local_sem.at[2]),
         pltpu.make_async_copy(w_value, w_in.at[:, pl.ds(nq + nk, nk)], local_sem.at[3]),
         pltpu.make_async_copy(w_out, w_o, local_sem.at[4]),
+        pltpu.make_async_copy(gain_in, gain, local_sem.at[5]),
+        pltpu.make_async_copy(select_in, select, local_sem.at[6]),
     ]
     for copy in copies:
         copy.start()
@@ -71,12 +73,17 @@
     for i in range(groups - 1):
         pl.semaphore_signal(barrier, inc=1, device_id={"tp": other(i)}, device_id_type=MESH)
 
-    def greet(i):
-        peer = lax.rem(me_kv + 1 + i, n_kv)
-        pl.semaphore_signal(barrier, inc=1, device_id={"kv": peer}, device_id_type=MESH)
-
-    loop(n_kv - 1, greet)
-    pl.semaphore_wait(barrier, groups + n_kv - 1)
+    @pl.when(me_kv > 0)
+    def _():
+        pl.semaphore_signal(barrier, inc=1, device_id={"kv": me_kv - 1}, device_id_type=MESH)
+
+    @pl.when(me_kv < n_kv - 1)
+    def _():
+        pl.semaphore_wait(barrier, groups + 1)
+
+    @pl.when(me_kv == n_kv - 1)
+    def _():
+        pl.semaphore_wait(barrier, groups)
 
     def piece(ref, slot, b):
         return ref.at[slot, pl.ds(b * QB, QB), :]
@@ -110,15 +117,24 @@
             tok_copy(i, b).start()
         mate_copy(b).start()
 
+    @pl.when(me_kv > 0)
+    def _():
+        pl.semaphore_wait(chain_sem, 1)
+
+    @pl.when(me_kv < n_kv - 1)
+    def _():
+        pl.semaphore_signal(
+            chain_sem, inc=1, device_id={"kv": me_kv + 1}, device_id_type=MESH)
+
     def sel_copy(peer):
         return pltpu.make_async_remote_copy(
-            src_ref=select, dst_ref=sel_all.at[me_kv],
+            src_ref=select_in, dst_ref=sel_all.at[me_kv],
             send_sem=sel_send.at[peer], recv_sem=sel_recv.at[me_kv],
             device_id={"kv": peer}, device_id_type=MESH)
 
     def sel_wait(peer):
         return pltpu.make_async_remote_copy(
-            src_ref=select, dst_ref=sel_all.at[peer],
+            src_ref=select_in, dst_ref=sel_all.at[peer],
             send_sem=sel_send.at[peer], recv_sem=sel_recv.at[peer],
             device_id={"kv": peer}, device_id_type=MESH)
 
@@ -141,6 +157,7 @@
         sin_s[b * QB:(b + 1) * QB, :] = jnp.where(lane < half, -sine, sine)
 
     chunks, chunk_owners, chunk_keys = bias_s.shape[0], recv_kv.shape[1], bias_s.shape[2]
+    copies[6].wait()
     listed = select[...]
 
     def bounds(ids, owner):
@@ -189,12 +206,13 @@
 
     loop(n_kv - 1, make_hot)
 
+    copies[5].wait()
     for copy in copies[:4]:
         copy.wait()
 
     def add_part(slot, b, acc, squares):
         part = tok[slot, pl.ds(b * QB, QB), :].astype(F32)
-        factor = gain[:, pl.ds(pl.multiple_of(slot * cols, cols), cols)].astype(F32)
+        factor = gain[pl.ds(pl.multiple_of(slot * cols, cols), cols)].astype(F32)[None, :]
         scaled = (part * factor).astype(BF16)
         weight = w_in[pl.ds(pl.multiple_of(slot * cols, cols), cols), :]
         acc = acc + jnp.dot(scaled, weight, preferred_element_type=F32)
@@ -417,9 +435,11 @@
     return pl.pallas_call(
         functools.partial(kernel, tp, n_kv),
         out_shape=jax.ShapeDtypeStruct((rows, w_out.shape[1]), jnp.bfloat16),
-        in_specs=[anywhere, fast, anywhere, anywhere, anywhere, anywhere, fast],
+        in_specs=[anywhere] * 7,
         out_specs=fast,
         scratch_shapes=[
+            pltpu.VMEM(gain.shape, BF16),
+            pltpu.VMEM(select.shape, jnp.int32),
             pltpu.VMEM((tp, rows, cols), BF16),
             pltpu.VMEM((tp, rows, nq), BF16),
             pltpu.VMEM((depth, nq + 2 * nk), BF16),
@@ -436,7 +456,7 @@
             pltpu.VMEM((n_kv, spec_rows, 2 * nk), BF16),
             pltpu.VMEM((chunks, chunk_owners, spec_rows, 2 * nk), BF16),
             pltpu.VMEM((chunks, blocks, chunk_owners * spec_rows), F32),
-            dma((5,)),
+            dma((7,)),
             dma((groups - 1, blocks)),
             dma((groups - 1, blocks)),
             dma((groups - 1, blocks)),
@@ -445,6 +465,7 @@
             dma((blocks,)),
             dma((n_kv,)),
             dma((n_kv,)),
+            pltpu.SemaphoreType.REGULAR,
             dma((n_kv,)),
             dma((n_kv,)),
             dma((groups - 1, blocks)),
@@ -455,8 +476,8 @@
             dma((blocks,)),
         ],
         compiler_params=pltpu.CompilerParams(
-            collective_id=0, has_side_effects=True, vmem_limit_bytes=60 * 1024 * 1024),
-    )(tokens, gain.reshape(1, -1), w_query, w_key, w_value, w_out, select)
+            collective_id=0, has_side_effects=True, vmem_limit_bytes=62914560),
+    )(tokens, gain, w_query, w_key, w_value, w_out, select)
 
 
 def solution(mesh):

time: 35.7 us -> 33.2 us (0.930)
  local copies, waits for them, and re-layouts: 3.16 us -> 1.87 us
  Pallas kernels: 32.3 us -> 31.2 us
    reshape x1 -> x0, local copies, waits for them, and re-layouts: 1.29 us -> none  [per_device(): gain.reshape(1, -1)]
    pallas_call x1, Pallas kernels: 32.3 us -> 31.2 us  [per_device(): pl.pallas_call(functools.partial(kernel, tp, n_kv), out_shape=jax.ShapeDt...]
where the time goes in v2:
time: 33.2 us; the launch traced here: 33.1 us
  Pallas kernels  31.2 us (94%)
  local copies, waits for them, and re-layouts  1.87 us (6%)
    pallas_call x1, Pallas kernels, per_device(): pl.pallas_call(functools.partial(kernel, tp, n_kv), out_shape=jax.ShapeDt...  31.2 us
    unnamed x1, local copies, waits for them, and re-layouts  1.87 us

profile of v2, /device:TPU:27, one launch (start us, length us, event | category | flops | bytes accessed | tf_op | source)
XLA Modules:
  0.0 33.1 jit_solution(6296241610807321229)
XLA Ops:
  0.0 31.2 %shard_map.73 = bf16[512,512]{1,0:T(8,128)(2,1)} custom-call(bf16[512,512]{1,0:T(8,128)(2,1)} %tokens.1, bf16[2048]{0:T(1024)(128)(2,1)} %gain_in.1, bf16[2048,256]{1,0:T(8,128)(2,1)} %w_query.1, bf16[2048,128]{1,0:T(8,128)(2,1)} %w_key.1, bf16[2048,128]{1,0:T(8,128)(2,1)} %w_value.1, bf16[1024,512]{1,0:T(8,128)(2,1)} %w_out.1, s32[4,32]{1,0:T(4,128)} %select_in.1), custom_call_target="tpu_custom_call" | custom-call | tf_op jit(solution)/shard_map/pallas_call | solution.py:435
  31.2 1.9 %copy.9 = bf16[512,512]{1,0:T(8,128)(2,1)} copy(bf16[512,512]{1,0:T(8,128)(2,1)} %shard_map.73) | data formatting | bytes 1048576

commit v3 on v2

--- a/solution.py
+++ b/solution.py
@@ -309,7 +309,7 @@
             device_id={"kv": peer}, device_id_type=MESH)
 
     def send_blocks(p):
-        peer = p + 1
+        peer = n_kv - 1 - p
 
         @pl.when(peer > me_kv)
         def _():
@@ -476,7 +476,7 @@
             dma((blocks,)),
         ],
         compiler_params=pltpu.CompilerParams(
-            collective_id=0, has_side_effects=True, vmem_limit_bytes=62914560),
+            collective_id=0, has_side_effects=True, vmem_limit_bytes=54400 * 1024),
     )(tokens, gain, w_query, w_key, w_value, w_out, select)
 
 

time: 33.2 us -> 32.9 us (level)
  the two profiles are of different devices: /device:TPU:27 before, /device:TPU:19 now
where the time goes in v3:
time: 32.9 us; the launch traced here: 32.7 us
  Pallas kernels  30.5 us (93%)
  local copies, waits for them, and re-layouts  2.16 us (7%)
    pallas_call x1, Pallas kernels, per_device(): pl.pallas_call(functools.partial(kernel, tp, n_kv), out_shape=jax.ShapeDt...  30.5 us
    unnamed x5, local copies, waits for them, and re-layouts  2.16 us

profile of v3, /device:TPU:19, one launch (start us, length us, event | category | flops | bytes accessed | tf_op | source)
XLA Modules:
  0.0 32.7 jit_solution(14276178311542505491)
XLA Ops:
  0.0 0.0 copy-start
  0.0 0.7 %copy-done = bf16[2048]{0:T(1024)(128)(2,1)S(1)} copy-done((bf16[2048]{0:T(1024)(128)(2,1)S(1)}, bf16[2048]{0:T(1024)(128)(2,1)}, u32[]{:S(2)}) %copy-start) | copy-done | bytes 4120
  0.7 0.0 copy-start.1
  0.7 0.7 %copy-done.1 = s32[4,32]{1,0:T(4,128)S(1)} copy-done((s32[4,32]{1,0:T(4,128)S(1)}, s32[4,32]{1,0:T(4,128)}, u32[]{:S(2)}) %copy-start.1) | copy-done | bytes 536
  1.4 30.5 %shard_map.73 = bf16[512,512]{1,0:T(8,128)(2,1)S(1)} custom-call(bf16[512,512]{1,0:T(8,128)(2,1)} %tokens.1, bf16[2048]{0:T(1024)(128)(2,1)S(1)} %copy-done, bf16[2048,256]{1,0:T(8,128)(2,1)} %w_query.1, bf16[2048,128]{1,0:T(8,128)(2,1)} %w_key.1, bf16[2048,128]{1,0:T(8,128)(2,1)} %w_value.1, bf16[1024,512]{1,0:T(8,128)(2,1)} %w_out.1, s32[4,32]{1,0:T(4,128)S(1)} %copy-done.1), custom_call_target="tpu_custom_call" | custom-call | tf_op jit(solution)/shard_map/pallas_call | solution.py:435
  31.9 0.8 %copy.9 = bf16[512,512]{1,0:T(8,128)(2,1)} copy(bf16[512,512]{1,0:T(8,128)(2,1)S(1)} %shard_map.73) | data formatting | bytes 1048576
Async XLA Ops:
  0.0 0.7 %copy-start = (bf16[2048]{0:T(1024)(128)(2,1)S(1)}, bf16[2048]{0:T(1024)(128)(2,1)}, u32[]{:S(2)}) copy-start(bf16[2048]{0:T(1024)(128)(2,1)} %gain_in.1) | copy-start | bytes 12292
  0.7 0.7 %copy-start.1 = (s32[4,32]{1,0:T(4,128)S(1)}, s32[4,32]{1,0:T(4,128)}, u32[]{:S(2)}) copy-start(s32[4,32]{1,0:T(4,128)} %select_in.1) | copy-start | bytes 1540
